TPU v7x, 32 devices: a whole 2x2x4 slice. The times are simulated.
32 devices in a mesh: fs: 8 (over z, y), tp: 4 (over x, core).
Axes of the slice: x: 2, y: 2, z: 4, core: 2. Of those that a mesh axis runs over, the one named last changes fastest.
Arguments:
- saved_inputs: bfloat16 [4096, 3072], P('fs'), may hold values from -6 to 6
- query_cotangent: bfloat16 [4096, 3072], P('fs', 'tp'), may hold values from -0.75 to 0.75
- attn_outputs: bfloat16 [4096, 3072], P('fs', 'tp'), may hold values from -6 to 6
- out_cotangent: bfloat16 [4096, 3072], P('fs'), may hold values from -0.75 to 0.75
- left_factor: bfloat16 [3072, 384], P('fs', 'tp'), may hold values from -0.109375 to 0.109375
- right_factor: bfloat16 [3072, 384], P('fs', 'tp'), may hold values from -0.109375 to 0.109375
- query_master: float32 [3072, 3072], P('fs', 'tp'), may hold values from -0.109375 to 0.109375
- out_master: float32 [3072, 3072], P('tp', 'fs'), may hold values from -0.109375 to 0.109375
- first_moment: float32 [2, 384, 3072], P(None, 'fs', 'tp'), may hold values from -14 to 14
- second_moment: float32 [2, 384, 3072], P(None, 'fs', 'tp'), may hold values from 0.3 to 3
Outputs:
- query_new: float32 [3072, 3072], P('fs', 'tp')
- out_new: float32 [3072, 3072], P('tp', 'fs')
- query_copy: bfloat16 [3072, 3072], P(None, 'tp')
- out_copy: bfloat16 [3072, 3072], P('tp')
- first_new: float32 [2, 384, 3072], P(None, 'fs', 'tp')
- second_new: float32 [2, 384, 3072], P(None, 'fs', 'tp')
All inputs are finite; a program needn't handle non-finite values.
Results may differ from a plain program's by a relative error of at most 0.0025.
Values may be sent and summed in bfloat16 or wider, within the bound.
A program may use at most 64 MiB of HBM per device.

v0:
```python
import jax
import jax.numpy as jnp
from jax import lax
from jax.sharding import PartitionSpec as P


def moment_step(first, second, grads):
    first_next = 0.9 * first + 0.1 * grads
    second_next = 0.99 * second + 0.01 * grads * grads
    return (first_next, second_next, first_next / (jnp.sqrt(second_next) + 1e-08))


def body(
    saved_inputs,
    query_cotangent,
    attn_outputs,
    out_cotangent,
    left_factor,
    right_factor,
    query_master,
    out_master,
    first_moment,
    second_moment,
):
    left_part = jnp.dot(
        saved_inputs,
        lax.all_gather(left_factor, "fs", axis=0, tiled=True),
        preferred_element_type=jnp.float32,
    )
    right_part = jnp.dot(
        out_cotangent,
        lax.all_gather(right_factor, "fs", axis=0, tiled=True),
        preferred_element_type=jnp.float32,
    )
    left_proj, right_proj, left_rows, right_rows = (
        lax.all_gather(left_part.astype(jnp.bfloat16), "tp", axis=1, tiled=True),
        lax.all_gather(right_part.astype(jnp.bfloat16), "tp", axis=1, tiled=True),
        lax.all_gather(left_factor, "tp", axis=1, tiled=True),
        lax.all_gather(right_factor, "tp", axis=1, tiled=True),
    )
    rows = first_moment.shape[1]
    dims = (((0,), (0,)), ((), ()))
    grad_query = lax.dot_general(
        left_proj, query_cotangent, dims, preferred_element_type=jnp.float32
    )
    grad_output = lax.dot_general(
        right_proj, attn_outputs, dims, preferred_element_type=jnp.float32
    )
    summed = lax.psum_scatter(
        jnp.stack([grad_query, grad_output], axis=1), "fs", scatter_dimension=0, tiled=True
    )
    grads = jnp.transpose(summed, (1, 0, 2))
    first_new, second_new, own_direction = moment_step(first_moment, second_moment, grads)
    direction_all = lax.all_gather(own_direction.astype(jnp.bfloat16), "fs", axis=1, tiled=True)
    squares = jnp.sum(own_direction * own_direction, axis=(1, 2))
    total = lax.psum(squares, ("fs", "tp"))
    entries = rows * lax.axis_size("fs") * own_direction.shape[2] * lax.axis_size("tp")
    scale = lax.rsqrt(total / entries + 1e-06)
    step_query = scale[0] * jnp.dot(left_rows, direction_all[0], preferred_element_type=jnp.float32)
    step_output = scale[1] * lax.dot_general(
        direction_all[1], right_rows, (((0,), (1,)), ((), ())), preferred_element_type=jnp.float32
    )
    query_new = query_master - 0.01 * step_query
    out_new = out_master - 0.01 * step_output
    query_copy, out_copy = (
        lax.all_gather(query_new.astype(jnp.bfloat16), "fs", axis=0, tiled=True),
        lax.all_gather(out_new.astype(jnp.bfloat16), "fs", axis=1, tiled=True),
    )
    return (query_new, out_new, query_copy, out_copy, first_new, second_new)


def solution(mesh):
    return jax.shard_map(
        body,
        mesh=mesh,
        in_specs=(
            P("fs", None),
            P("fs", "tp"),
            P("fs", "tp"),
            P("fs", None),
            P("fs", "tp"),
            P("fs", "tp"),
            P("fs", "tp"),
            P("tp", "fs"),
            P(None, "fs", "tp"),
            P(None, "fs", "tp"),
        ),
        out_specs=(
            P("fs", "tp"),
            P("tp", "fs"),
            P(None, "tp"),
            P("tp", None),
            P(None, "fs", "tp"),
            P(None, "fs", "tp"),
        ),
        check_vma=False,
    )
```

profile of v0, /device:TPU:0, one launch (start us, length us, event | category | flops | bytes accessed | tf_op | source)
XLA Modules:
  0.0 390.2 jit_solution(14397979788832499997)
XLA Ops:
  7.2 0.0 reduce-scatter.2.cloned.1.call-start
  7.2 33.9 %all_gather.27 = bf16[3072,96]{0,1:T(8,128)(2,1)S(1)} all-gather(bf16[384,96]{0,1:T(8,128)(2,1)} %param.14), channel_id=1, replica_groups=mesh['fs'=8,'tp'=4] {'fs'}, dimensions={0}, use_global_device_ids=true | all-gather | bytes 663552 | tf_op jit(solution)/shard_map/all_gather | solution.py:27
  41.1 1.1 convolution_convert_fusion.1
  42.2 6.5 %all_gather.28 = bf16[512,384]{0,1:T(8,128)(2,1)S(1)} all-gather(bf16[512,96]{0,1:T(8,128)(2,1)S(1)} %convolution_convert_fusion.1), channel_id=1, replica_groups=mesh['fs'=8,'tp'=4] {'tp'}, dimensions={1}, use_global_device_ids=true | all-gather | bytes 491520 | tf_op jit(solution)/shard_map/all_gather | solution.py:36
  48.7 31.5 %all_gather.29 = bf16[3072,96]{0,1:T(8,128)(2,1)S(1)} all-gather(bf16[384,96]{0,1:T(8,128)(2,1)S(1)} %copy-done.8), channel_id=1, replica_groups=mesh['fs'=8,'tp'=4] {'fs'}, dimensions={0}, use_global_device_ids=true | all-gather | bytes 663552 | tf_op jit(solution)/shard_map/all_gather | solution.py:32
  80.2 1.1 convolution_convert_fusion
  81.3 6.1 %all_gather.30 = bf16[512,384]{0,1:T(8,128)(2,1)S(1)} all-gather(bf16[512,96]{0,1:T(8,128)(2,1)S(1)} %convolution_convert_fusion), channel_id=1, replica_groups=mesh['fs'=8,'tp'=4] {'tp'}, dimensions={1}, use_global_device_ids=true | all-gather | bytes 491520 | tf_op jit(solution)/shard_map/all_gather | solution.py:37
  87.5 0.5 convolution_bitcast_fusion
  87.9 0.7 copy-done.5
  88.6 0.5 convolution_bitcast_fusion.1
  89.1 1.6 pad_maximum_fusion
  90.6 0.0 reduce-scatter.2.cloned.1.call-update
  90.7 0.0 all-gather.4.cloned.1.call-start
  90.7 70.5 %reduce-scatter.2.cloned.1.call-done = f32[48,2,768]{2,0,1:T(8,128)} async-done(((f32[384,2,768]{2,0,1:T(8,128)}), f32[48,2,768]{2,0,1:T(8,128)}) %reduce-scatter.2.cloned.1.call-update) | async-done | bytes 294928 | tf_op jit(solution)/shard_map/reduce_scatter | solution.py:49
  161.2 1.3 multiply_reduce_fusion
  162.6 0.7 copy-done.2
  163.3 0.1 copy-done.3
  163.4 0.8 fusion.7
  164.2 0.0 all-gather.6.cloned.1.call-start
  164.3 2.7 copy.19
  166.9 5.9 %all_gather.32 = bf16[384,384]{0,1:T(8,128)(2,1)S(1)} all-gather(bf16[384,96]{0,1:T(8,128)(2,1)S(1)} %copy-done.7), channel_id=1, replica_groups=mesh['fs'=8,'tp'=4] {'tp'}, dimensions={1}, use_global_device_ids=true | all-gather | bytes 368640 | tf_op jit(solution)/shard_map/all_gather | solution.py:38
  172.8 40.3 %psum.7 = f32[2]{0:T(128)S(1)} all-reduce(f32[2]{0:T(128)S(1)} %get-tuple-element.18), channel_id=1, replica_groups=mesh['fs'=8,'tp'=4] {'fs','tp'}, use_global_device_ids=true, to_apply=%region_2.0 | all-reduce | flops 2 | bytes 16 | tf_op jit(solution)/shard_map/psum | solution.py:56
  213.1 0.6 fusion.10
  213.7 3.8 fusion.11
  217.5 0.0 all-gather.8.cloned.1.call-start
  217.6 6.7 %all_gather.33 = bf16[384,384]{0,1:T(8,128)(2,1)S(1)} all-gather(bf16[384,96]{0,1:T(8,128)(2,1)S(1)} %copy-done.9), channel_id=1, replica_groups=mesh['fs'=8,'tp'=4] {'tp'}, dimensions={1}, use_global_device_ids=true | all-gather | bytes 368640 | tf_op jit(solution)/shard_map/all_gather | solution.py:39
  224.3 3.9 fusion.12
  228.2 2.7 copy.20
  230.9 67.2 %all-gather.6.cloned.1.call-done = bf16[3072,768]{0,1:T(8,128)(2,1)} async-done(((bf16[384,768]{0,1:T(8,128)(2,1)}), bf16[3072,768]{0,1:T(8,128)(2,1)}) %all-gather.6.cloned.1.call-update) | async-done | bytes 4718608 | tf_op jit(solution)/shard_map/all_gather | solution.py:66
  298.1 6.6 %copy.21 = bf16[3072,768]{1,0:T(8,128)(2,1)} copy(bf16[3072,768]{0,1:T(8,128)(2,1)} %all-gather.6.cloned.1.call-done) | data formatting | bytes 9437184
  304.7 74.1 %all-gather.8.cloned.1.call-done = bf16[768,3072]{1,0:T(8,128)(2,1)} async-done(((bf16[768,384]{1,0:T(8,128)(2,1)}), bf16[768,3072]{1,0:T(8,128)(2,1)}) %all-gather.8.cloned.1.call-update) | async-done | bytes 4718608 | tf_op jit(solution)/shard_map/all_gather | solution.py:67
  378.8 4.8 %copy.23 = bf16[768,3072]{1,0:T(8,128)(2,1)} copy(bf16[768,3072]{1,0:T(8,128)(2,1)} %all-gather.8.cloned.1.call-done) | data formatting | bytes 9437184
  (22 shorter events, 0.1 us)
Async XLA Ops:
  7.2 33.9 %copy-start = (bf16[512,3072]{1,0:T(8,128)(2,1)S(1)}, bf16[512,3072]{1,0:T(8,128)(2,1)}, u32[]{:S(2)}) copy-start(bf16[512,3072]{1,0:T(8,128)(2,1)} %param.10) | copy-start | bytes 9437188
  7.2 154.1 %reduce-scatter.2.cloned.1.call-start = ((), (), s32[]{:S(2)}) async-start(), calls=%async_computation.1 | async-start | bytes 2654208 | tf_op jit(solution)/shard_map/reduce_scatter | solution.py:49
  41.1 7.6 %copy-start.8 = (bf16[384,96]{0,1:T(8,128)(2,1)S(1)}, bf16[384,96]{0,1:T(8,128)(2,1)}, u32[]{:S(2)}) copy-start(bf16[384,96]{0,1:T(8,128)(2,1)} %param.15) | copy-start | bytes 221188
  41.1 39.1 %copy-start.1 = (bf16[512,3072]{1,0:T(8,128)(2,1)S(1)}, bf16[512,3072]{1,0:T(8,128)(2,1)}, u32[]{:S(2)}) copy-start(bf16[512,3072]{1,0:T(8,128)(2,1)} %param.13) | copy-start | bytes 9437188
  80.2 7.3 %copy-start.4 = (bf16[512,768]{1,0:T(8,128)(2,1)S(1)}, bf16[512,768]{1,0:T(8,128)(2,1)}, u32[]{:S(2)}) copy-start(bf16[512,768]{1,0:T(8,128)(2,1)} %param.12) | copy-start | bytes 2359300
  87.5 1.1 copy-start.5
  90.6 70.6 %copy-start.6 = (f32[2,48,768]{2,1,0:T(8,128)S(1)}, f32[2,48,768]{2,1,0:T(8,128)}, u32[]{:S(2)}) copy-start(f32[2,48,768]{2,1,0:T(8,128)} %param.19) | copy-start | bytes 884740
  90.7 123.0 %all-gather.4.cloned.1.call-start = ((), (), s32[]{:S(2)}) async-start(), calls=%async_computation.2 | async-start | bytes 1327104 | tf_op jit(solution)/shard_map/all_gather | solution.py:54
  162.6 0.7 copy-start.2
  162.6 0.8 copy-start.3
  164.2 2.7 copy-start.7
  164.2 133.9 %all-gather.6.cloned.1.call-start = ((), (), s32[]{:S(2)}) async-start(), calls=%async_computation.3 | async-start | bytes 5308416 | tf_op jit(solution)/shard_map/all_gather | solution.py:66
  213.7 3.9 %copy-start.9 = (bf16[384,96]{0,1:T(8,128)(2,1)S(1)}, bf16[384,96]{0,1:T(8,128)(2,1)}, u32[]{:S(2)}) copy-start(bf16[384,96]{0,1:T(8,128)(2,1)} %param.15) | copy-start | bytes 221188
  217.5 161.2 %all-gather.8.cloned.1.call-start = ((), (), s32[]{:S(2)}) async-start(), calls=%async_computation.4 | async-start | bytes 5308416 | tf_op jit(solution)/shard_map/all_gather | solution.py:67
Sparse Core Ops, SparseCore 0:
  90.8 70.4 reduce-scatter.1
  164.3 40.5 all-gather.3
  217.7 80.3 all-gather.5
  300.0 78.7 all-gather.7
where the time goes:
time: 391 us; the launch traced here: 390 us
  waiting for transfers between devices  212 us (54%)
  blocking collectives  131 us (34%)
  local copies, waits for them, and re-layouts  18.8 us (5%)
  between operations  13.8 us (4%)
  matrix products  10.9 us (3%)
    all_gather x1, waiting for transfers between devices, body(): lax.all_gather(out_new.astype(jnp.bfloat16), 'fs', axis=1, tiled=True)  74.1 us
    reduce_scatter x1, waiting for transfers between devices, body(): lax.psum_scatter(jnp.stack([grad_query, grad_output], axis=1), 'fs', scat...  70.5 us
    all_gather x1, waiting for transfers between devices, body(): lax.all_gather(query_new.astype(jnp.bfloat16), 'fs', axis=0, tiled=True)  67.2 us
    psum x1, blocking collectives, body(): total = lax.psum(squares, ('fs', 'tp'))  40.3 us
    all_gather x1, blocking collectives, body(): lax.all_gather(left_factor, 'fs', axis=0, tiled=True)  33.9 us
    all_gather x1, blocking collectives, body(): lax.all_gather(right_factor, 'fs', axis=0, tiled=True)  31.5 us
    unnamed x24, local copies, waits for them, and re-layouts  18.3 us
  transfers between devices with their start and end apart: 4, of which 3 were waited for; matrix products, arithmetic and copies ran while one was open for 4% of the time, Pallas kernels for 0%

commit v1 on v0

--- a/solution.py
+++ b/solution.py
@@ -53,7 +53,7 @@
     first_new, second_new, own_direction = moment_step(first_moment, second_moment, grads)
     direction_all = lax.all_gather(own_direction.astype(jnp.bfloat16), "fs", axis=1, tiled=True)
     squares = jnp.sum(own_direction * own_direction, axis=(1, 2))
-    total = lax.psum(squares, ("fs", "tp"))
+    total = lax.psum(lax.psum(squares, "tp"), "fs")
     entries = rows * lax.axis_size("fs") * own_direction.shape[2] * lax.axis_size("tp")
     scale = lax.rsqrt(total / entries + 1e-06)
     step_query = scale[0] * jnp.dot(left_rows, direction_all[0], preferred_element_type=jnp.float32)

time: 391 us -> 381 us (0.974)
  blocking collectives: 131 us -> 116 us
  waiting for transfers between devices: 212 us -> 216 us
    psum x1 -> x2, blocking collectives: 40.3 us -> 26.5 us  [body(): total = lax.psum(lax.psum(squares, 'tp'), 'fs')]
    all_gather x1, waiting for transfers between devices: 0.01 us -> 4.88 us  [body(): lax.all_gather(own_direction.astype(jnp.bfloat16), 'fs', axis=1, tiled=True)]
  transfers between devices with their start and end apart: 4 -> 4, of which waited for: 3 -> 4; matrix products, arithmetic and copies ran while one was open for 4% -> 4% of each run, Pallas kernels for 0% -> 0%
where the time goes in v1:
time: 381 us; the launch traced here: 380 us
  waiting for transfers between devices  216 us (57%)
  blocking collectives  116 us (30%)
  local copies, waits for them, and re-layouts  18.9 us (5%)
  between operations  13.8 us (4%)
  matrix products  10.9 us (3%)
    all_gather x1, waiting for transfers between devices, body(): lax.all_gather(out_new.astype(jnp.bfloat16), 'fs', axis=1, tiled=True)  74.1 us
    reduce_scatter x1, waiting for transfers between devices, body(): lax.psum_scatter(jnp.stack([grad_query, grad_output], axis=1), 'fs', scat...  70.5 us
    all_gather x1, waiting for transfers between devices, body(): lax.all_gather(query_new.astype(jnp.bfloat16), 'fs', axis=0, tiled=True)  66.9 us
    all_gather x1, blocking collectives, body(): lax.all_gather(left_factor, 'fs', axis=0, tiled=True)  33.9 us
    all_gather x1, blocking collectives, body(): lax.all_gather(right_factor, 'fs', axis=0, tiled=True)  31.5 us
    psum x2, blocking collectives, body(): total = lax.psum(lax.psum(squares, 'tp'), 'fs')  26.5 us
    unnamed x24, local copies, waits for them, and re-layouts  18.3 us
  transfers between devices with their start and end apart: 4, of which 4 were waited for; matrix products, arithmetic and copies ran while one was open for 4% of the time, Pallas kernels for 0%

profile of v1, /device:TPU:0, one launch (start us, length us, event | category | flops | bytes accessed | tf_op | source)
XLA Modules:
  0.0 380.3 jit_solution(9525001210661544813)
XLA Ops:
  7.2 33.9 %all_gather.27 = bf16[3072,96]{0,1:T(8,128)(2,1)S(1)} all-gather(bf16[384,96]{0,1:T(8,128)(2,1)} %param.14), channel_id=1, replica_groups=mesh['fs'=8,'tp'=4] {'fs'}, dimensions={0}, use_global_device_ids=true | all-gather | bytes 663552 | tf_op jit(solution)/shard_map/all_gather | solution.py:27
  41.1 1.1 convolution_convert_fusion.1
  42.2 6.5 %all_gather.28 = bf16[512,384]{0,1:T(8,128)(2,1)S(1)} all-gather(bf16[512,96]{0,1:T(8,128)(2,1)S(1)} %convolution_convert_fusion.1), channel_id=1, replica_groups=mesh['fs'=8,'tp'=4] {'tp'}, dimensions={1}, use_global_device_ids=true | all-gather | bytes 491520 | tf_op jit(solution)/shard_map/all_gather | solution.py:36
  48.7 31.5 %all_gather.29 = bf16[3072,96]{0,1:T(8,128)(2,1)S(1)} all-gather(bf16[384,96]{0,1:T(8,128)(2,1)S(1)} %copy-done.8), channel_id=1, replica_groups=mesh['fs'=8,'tp'=4] {'fs'}, dimensions={0}, use_global_device_ids=true | all-gather | bytes 663552 | tf_op jit(solution)/shard_map/all_gather | solution.py:32
  80.2 1.1 convolution_convert_fusion
  81.3 6.1 %all_gather.30 = bf16[512,384]{0,1:T(8,128)(2,1)S(1)} all-gather(bf16[512,96]{0,1:T(8,128)(2,1)S(1)} %convolution_convert_fusion), channel_id=1, replica_groups=mesh['fs'=8,'tp'=4] {'tp'}, dimensions={1}, use_global_device_ids=true | all-gather | bytes 491520 | tf_op jit(solution)/shard_map/all_gather | solution.py:37
  87.5 0.5 convolution_bitcast_fusion
  87.9 0.7 copy-done.5
  88.6 0.5 convolution_bitcast_fusion.1
  89.1 1.6 pad_maximum_fusion
  90.7 0.0 all-gather.4.cloned.1.call-start
  90.7 70.5 %reduce-scatter.2.cloned.1.call-done = f32[48,2,768]{2,0,1:T(8,128)} async-done(((f32[384,2,768]{2,0,1:T(8,128)}), f32[48,2,768]{2,0,1:T(8,128)}) %reduce-scatter.2.cloned.1.call-update) | async-done | bytes 294928 | tf_op jit(solution)/shard_map/reduce_scatter | solution.py:49
  161.2 1.3 multiply_reduce_fusion
  162.6 0.7 copy-done.2
  163.3 0.1 copy-done.3
  163.4 0.8 fusion.7
  164.2 0.0 all-gather.6.cloned.1.call-start
  164.2 5.9 %all_gather.32 = bf16[384,384]{0,1:T(8,128)(2,1)S(1)} all-gather(bf16[384,96]{0,1:T(8,128)(2,1)S(1)} %copy-done.7), channel_id=1, replica_groups=mesh['fs'=8,'tp'=4] {'tp'}, dimensions={1}, use_global_device_ids=true | all-gather | bytes 368640 | tf_op jit(solution)/shard_map/all_gather | solution.py:38
  170.2 7.4 %psum.14 = f32[2]{0:T(128)S(1)} all-reduce(f32[2]{0:T(128)S(1)} %get-tuple-element.18), channel_id=1, replica_groups=mesh['fs'=8,'tp'=4] {'tp'}, use_global_device_ids=true, to_apply=%region_2.0 | all-reduce | flops 2 | bytes 16 | tf_op jit(solution)/shard_map/psum | solution.py:56
  177.6 2.7 copy.19
  180.2 19.1 %psum.15 = f32[2]{0:T(128)S(1)} all-reduce(f32[2]{0:T(128)S(1)} %psum.14), channel_id=1, replica_groups=mesh['fs'=8,'tp'=4] {'fs'}, use_global_device_ids=true, to_apply=%region_3.0 | all-reduce | flops 2 | bytes 16 | tf_op jit(solution)/shard_map/psum | solution.py:56
  199.3 0.6 fusion.10
  199.9 4.9 %all-gather.4.cloned.1.call-done = bf16[2,384,768]{2,1,0:T(8,128)(2,1)} async-done(((bf16[2,48,768]{2,1,0:T(8,128)(2,1)}), bf16[2,384,768]{2,1,0:T(8,128)(2,1)}) %all-gather.4.cloned.1.call-update) | async-done | bytes 1179664 | tf_op jit(solution)/shard_map/all_gather | solution.py:54
  204.8 3.9 %fusion.11 = (bf16[384,768]{0,1:T(8,128)(2,1)}, f32[384,768]{0,1:T(8,128)}) fusion(f32[384,768]{0,1:T(8,128)} %copy.19, bf16[384,384]{0,1:T(8,128)(2,1)S(1)} %all_gather.32, bf16[2,384,768]{2,1,0:T(8,128)(2,1)} %all-gather.4.cloned.1.call-done, f32[]{:T(128)} %bitcast.3), kind=kOutput, calls=%fused_computation.23 | convolution fusion | flops 227672064 | bytes 3834368 | tf_op jit(solution)/shard_map/dot_general | solution.py:59
  208.8 0.0 all-gather.8.cloned.1.call-start
  208.8 5.9 %all_gather.33 = bf16[384,384]{0,1:T(8,128)(2,1)S(1)} all-gather(bf16[384,96]{0,1:T(8,128)(2,1)S(1)} %copy-done.9), channel_id=1, replica_groups=mesh['fs'=8,'tp'=4] {'tp'}, dimensions={1}, use_global_device_ids=true | all-gather | bytes 368640 | tf_op jit(solution)/shard_map/all_gather | solution.py:39
  214.7 3.9 %fusion.12 = (bf16[768,384]{1,0:T(8,128)(2,1)}, f32[768,384]{1,0:T(8,128)}) fusion(f32[768,384]{1,0:T(8,128)} %param.17, bf16[384,384]{0,1:T(8,128)(2,1)S(1)} %all_gather.33, bf16[2,384,768]{2,1,0:T(8,128)(2,1)} %all-gather.4.cloned.1.call-done, f32[]{:T(128)} %bitcast.6), kind=kOutput, calls=%fused_computation.24 | convolution fusion | flops 227672064 | bytes 3834368 | tf_op jit(solution)/shard_map/dot_general | solution.py:60
  218.6 2.7 copy.20
  221.3 66.9 %all-gather.6.cloned.1.call-done = bf16[3072,768]{0,1:T(8,128)(2,1)} async-done(((bf16[384,768]{0,1:T(8,128)(2,1)}), bf16[3072,768]{0,1:T(8,128)(2,1)}) %all-gather.6.cloned.1.call-update) | async-done | bytes 4718608 | tf_op jit(solution)/shard_map/all_gather | solution.py:66
  288.2 6.6 %copy.21 = bf16[3072,768]{1,0:T(8,128)(2,1)} copy(bf16[3072,768]{0,1:T(8,128)(2,1)} %all-gather.6.cloned.1.call-done) | data formatting | bytes 9437184
  294.8 74.1 %all-gather.8.cloned.1.call-done = bf16[768,3072]{1,0:T(8,128)(2,1)} async-done(((bf16[768,384]{1,0:T(8,128)(2,1)}), bf16[768,3072]{1,0:T(8,128)(2,1)}) %all-gather.8.cloned.1.call-update) | async-done | bytes 4718608 | tf_op jit(solution)/shard_map/all_gather | solution.py:67
  368.9 4.8 %copy.23 = bf16[768,3072]{1,0:T(8,128)(2,1)} copy(bf16[768,3072]{1,0:T(8,128)(2,1)} %all-gather.8.cloned.1.call-done) | data formatting | bytes 9437184
  (23 shorter events, 0.2 us)
Async XLA Ops:
  7.2 33.9 %copy-start = (bf16[512,3072]{1,0:T(8,128)(2,1)S(1)}, bf16[512,3072]{1,0:T(8,128)(2,1)}, u32[]{:S(2)}) copy-start(bf16[512,3072]{1,0:T(8,128)(2,1)} %param.10) | copy-start | bytes 9437188
  7.2 154.1 %reduce-scatter.2.cloned.1.call-start = ((), (), s32[]{:S(2)}) async-start(), calls=%async_computation.1 | async-start | bytes 2654208 | tf_op jit(solution)/shard_map/reduce_scatter | solution.py:49
  41.1 7.6 %copy-start.8 = (bf16[384,96]{0,1:T(8,128)(2,1)S(1)}, bf16[384,96]{0,1:T(8,128)(2,1)}, u32[]{:S(2)}) copy-start(bf16[384,96]{0,1:T(8,128)(2,1)} %param.15) | copy-start | bytes 221188
  41.1 39.1 %copy-start.1 = (bf16[512,3072]{1,0:T(8,128)(2,1)S(1)}, bf16[512,3072]{1,0:T(8,128)(2,1)}, u32[]{:S(2)}) copy-start(bf16[512,3072]{1,0:T(8,128)(2,1)} %param.13) | copy-start | bytes 9437188
  80.2 7.3 %copy-start.4 = (bf16[512,768]{1,0:T(8,128)(2,1)S(1)}, bf16[512,768]{1,0:T(8,128)(2,1)}, u32[]{:S(2)}) copy-start(bf16[512,768]{1,0:T(8,128)(2,1)} %param.12) | copy-start | bytes 2359300
  87.5 1.1 copy-start.5
  90.6 70.6 %copy-start.6 = (f32[2,48,768]{2,1,0:T(8,128)S(1)}, f32[2,48,768]{2,1,0:T(8,128)}, u32[]{:S(2)}) copy-start(f32[2,48,768]{2,1,0:T(8,128)} %param.19) | copy-start | bytes 884740
  90.7 73.6 %copy-start.7 = (bf16[384,96]{0,1:T(8,128)(2,1)S(1)}, bf16[384,96]{0,1:T(8,128)(2,1)}, u32[]{:S(2)}) copy-start(bf16[384,96]{0,1:T(8,128)(2,1)} %param.14) | copy-start | bytes 221188
  90.7 114.1 %all-gather.4.cloned.1.call-start = ((), (), s32[]{:S(2)}) async-start(), calls=%async_computation.2 | async-start | bytes 1327104 | tf_op jit(solution)/shard_map/all_gather | solution.py:54
  162.6 0.7 copy-start.2
  162.6 0.8 copy-start.3
  164.2 124.0 %all-gather.6.cloned.1.call-start = ((), (), s32[]{:S(2)}) async-start(), calls=%async_computation.3 | async-start | bytes 5308416 | tf_op jit(solution)/shard_map/all_gather | solution.py:66
  204.8 4.0 %copy-start.9 = (bf16[384,96]{0,1:T(8,128)(2,1)S(1)}, bf16[384,96]{0,1:T(8,128)(2,1)}, u32[]{:S(2)}) copy-start(bf16[384,96]{0,1:T(8,128)(2,1)} %param.15) | copy-start | bytes 221188
  208.8 160.1 %all-gather.8.cloned.1.call-start = ((), (), s32[]{:S(2)}) async-start(), calls=%async_computation.4 | async-start | bytes 5308416 | tf_op jit(solution)/shard_map/all_gather | solution.py:67
Sparse Core Ops, SparseCore 0:
  90.8 70.4 reduce-scatter.1
  164.3 40.4 all-gather.3
  208.9 79.2 all-gather.5
  290.1 78.7 all-gather.7
